TPU v7x, 32 devices: a whole 2x2x4 slice. The times are simulated.
32 devices in a mesh: grp: 2 (over x), fs: 4 (over z), tp: 4 (over y, core).
Axes of the slice: x: 2, y: 2, z: 4, core: 2. Of those that a mesh axis runs over, the one named last changes fastest.
Arguments:
- tokens: bfloat16 [960, 2048], P(('grp', 'tp')), parts along dimension 0, may hold values from -60 to 60
- route_expert: int32 [960, 4], P(('grp', 'tp')), parts along dimension 0, may hold values from 0 to 31, all different within a row; in each aligned block of 120 rows (0 to 119, 120 to 239, ...) at most 16 rows name the same one
- route_weight: float32 [960, 4], P(('grp', 'tp')), parts along dimension 0, may hold values from 0.05 to 1
- norm_gain: float32 [2048], P('tp'), may hold values from 0.1 to 1.9
- gate_train: float32 [32, 2048, 2048], P(None, 'tp', 'fs'), may hold values from -8 to 8
- up_train: float32 [32, 2048, 2048], P(None, 'tp', 'fs'), may hold values from -8 to 8
- down_train: float32 [32, 2048, 2048], P(None, 'tp', 'fs'), may hold values from -0.013671875 to 0.013671875
Outputs:
- gate_serve: bfloat16 [64, 2048, 2048], P(('grp', 'tp'), None, 'fs'), parts along dimension 0
- up_serve: bfloat16 [64, 2048, 2048], P(('grp', 'tp'), None, 'fs'), parts along dimension 0
- down_serve: bfloat16 [64, 2048, 2048], P(('grp', 'tp'), None, 'fs'), parts along dimension 0
- mixed: bfloat16 [960, 2048], P(('grp', 'tp'), 'fs'), parts along dimension 0
There are 2 independent parts, one for each index of `grp`. A program takes and returns all parts, laid end to end along the dimension named above; an argument that names none is the same for every part. Nothing has to cross between parts.
Inputs may be any that keep to these rules, and one draw needn't show every extreme that they name: `route_expert`: each row names 4 different experts; the rows of one device name each expert at most 16 times.
All inputs are finite; a program needn't handle non-finite values.
Results may differ from a plain program's by a relative error of at most 0.0087.
Values may be sent and summed in bfloat16 or wider, within the bound.
A program may use at most 320 MiB of HBM per device.

v0:
```python
import jax
import jax.numpy as jnp
from jax import lax
from jax.sharding import PartitionSpec as P

EXPERTS = 32
TOP = 4
CAP = 16


def activate(gate_pre, up_pre):
    clamped = jnp.minimum(gate_pre, 7.0)
    bounded = jnp.clip(up_pre, -7.0, 7.0)
    return (clamped * jax.nn.sigmoid(1.702 * clamped) * (bounded + 1.0)).astype(jnp.bfloat16)


def local(tokens, route_expert, route_weight, norm_gain, gate_train, up_train, down_train):
    gate_local = (gate_train * norm_gain[None, :, None]).astype(jnp.bfloat16)
    up_local = (up_train * norm_gain[None, :, None]).astype(jnp.bfloat16)
    down_local = down_train.astype(jnp.bfloat16)
    gate_serve, up_serve, down_serve = (
        lax.all_to_all(gate_local, "tp", split_axis=0, concat_axis=1, tiled=True),
        lax.all_to_all(up_local, "tp", split_axis=0, concat_axis=1, tiled=True),
        lax.all_to_all(down_local, "tp", split_axis=0, concat_axis=1, tiled=True),
    )
    tp_count = lax.axis_size("tp")
    fs_count = lax.axis_size("fs")
    per_dev = EXPERTS // tp_count
    tok_rows = tokens.shape[0]
    floated = tokens.astype(jnp.float32)
    normed = (
        floated * lax.rsqrt(jnp.mean(floated * floated, axis=-1, keepdims=True) + 1e-06)
    ).astype(jnp.bfloat16)
    flat_expert = route_expert.reshape(-1)
    expert_ids = jnp.arange(EXPERTS, dtype=jnp.int32)
    onehot = (flat_expert[:, None] == expert_ids[None, :]).astype(jnp.int32)
    slot_rank = jnp.sum((jnp.cumsum(onehot, axis=0) - 1) * onehot, axis=1)
    slot_index = flat_expert * CAP + slot_rank
    slot_hit = slot_index[:, None] == jnp.arange(EXPERTS * CAP, dtype=jnp.int32)[None, :]
    placement = slot_hit.reshape(tok_rows, TOP, EXPERTS * CAP).astype(jnp.float32)
    scatter_mat = jnp.sum(placement, axis=1).astype(jnp.bfloat16)
    combine_mat = jnp.sum(placement * route_weight[:, :, None], axis=1)
    col_width = normed.shape[1] // fs_count
    my_block = lax.axis_index("fs")
    column_part = lax.dynamic_slice_in_dim(normed, my_block * col_width, col_width, 1)
    buffer = lax.dot_general(
        scatter_mat, column_part, (((0,), (0,)), ((), ())), preferred_element_type=jnp.float32
    )
    arrived = lax.all_to_all(
        buffer.astype(jnp.bfloat16).reshape(EXPERTS, CAP, column_part.shape[1]),
        "tp",
        split_axis=0,
        concat_axis=0,
        tiled=True,
    )
    arrived = arrived.reshape(tp_count, per_dev, CAP, col_width)
    block_in = lax.all_gather(arrived, "fs", axis=3, tiled=True)
    gate_part = jnp.einsum(
        "secd,edf->secf", block_in, gate_serve, preferred_element_type=jnp.float32
    )
    up_part = jnp.einsum("secd,edf->secf", block_in, up_serve, preferred_element_type=jnp.float32)
    hidden = activate(gate_part, up_part)
    expert_out = jnp.einsum(
        "secf,efd->secd",
        lax.all_gather(hidden, "fs", axis=3, tiled=True),
        down_serve,
        preferred_element_type=jnp.float32,
    ).astype(jnp.bfloat16)
    outgoing = expert_out.reshape(tp_count * per_dev, CAP, down_serve.shape[2])
    returned_rows = lax.all_to_all(outgoing, "tp", split_axis=0, concat_axis=0, tiled=True).reshape(
        EXPERTS * CAP, down_serve.shape[2]
    )
    mixed = jnp.dot(
        combine_mat, returned_rows.astype(jnp.float32), precision=lax.Precision.HIGHEST
    ).astype(jnp.bfloat16)
    return (gate_serve, up_serve, down_serve, mixed)


def solution(mesh):
    return jax.shard_map(
        local,
        mesh=mesh,
        in_specs=(
            P(("grp", "tp"), None),
            P(("grp", "tp"), None),
            P(("grp", "tp"), None),
            P("tp"),
            P(None, "tp", "fs"),
            P(None, "tp", "fs"),
            P(None, "tp", "fs"),
        ),
        out_specs=(
            P(("grp", "tp"), None, "fs"),
            P(("grp", "tp"), None, "fs"),
            P(("grp", "tp"), None, "fs"),
            P(("grp", "tp"), "fs"),
        ),
        check_vma=False,
    )
```

profile of v0, /device:TPU:0, one launch (start us, length us, event | category | flops | bytes accessed | tf_op | source)
XLA Modules:
  0.0 668.9 jit_solution(10352614119127516276)
XLA Ops:
  7.2 1.1 convert_element_type.44
  8.3 1.2 multiply_reduce_fusion
  9.5 0.8 copy.41
  10.3 0.1 eq.36
  10.5 1.2 reduce-window.6
  11.6 0.2 slice_reduce_fusion
  11.9 0.1 bitcast_bitcast_fusion
  12.0 0.1 reduce_sum.39
  12.1 0.1 copy.44
  12.2 0.7 multiply_add_fusion
  12.9 0.9 convert_reduce_fusion
  13.9 1.2 convolution_convert_fusion
  15.0 4.3 all-to-all-start.3
  19.3 33.2 %multiply_convert_fusion = (bf16[32,512,512]{2,1,0:T(8,128)(2,1)}, bf16[32,512,512]{2,1,0:T(8,128)(2,1)}) fusion(f32[32,512,512]{2,1,0:T(8,128)} %param.12, f32[512]{0:T(512)} %param.10, f32[32,512,512]{2,1,0:T(8,128)} %param.11), kind=kLoop, calls=%fused_computation | loop fusion | flops 33554432 | bytes 100665344 | tf_op jit(solution)/shard_map/convert_element_type | solution.py:19
  52.5 194.1 %all_to_all.64 = bf16[32,512,512]{2,1,0:T(8,128)(2,1)} all-to-all(bf16[32,512,512]{2,1,0:T(8,128)(2,1)} %get-tuple-element.7), channel_id=1, replica_groups=mesh['grp'=2,'fs'=4,'tp'=4] {'tp'}, dimensions={0} | all-to-all | bytes 33554432 | tf_op jit(solution)/shard_map/all_to_all | solution.py:22
  246.6 7.1 %all-to-all-start.1 = ((bf16[32,512,512]{2,1,0:T(8,128)(2,1)}), bf16[32,512,512]{2,1,0:T(8,128)(2,1)}, u32[]{:S(2)}, u32[]{:S(2)}) async-start(bf16[32,512,512]{2,1,0:T(8,128)(2,1)} %get-tuple-element.6), calls=%async_computation.1 | async-start | bytes 33554432 | tf_op jit(solution)/shard_map/all_to_all | solution.py:23
  253.7 17.3 %convert_element_type.41 = bf16[32,512,512]{2,1,0:T(8,128)(2,1)} convert(f32[32,512,512]{2,1,0:T(8,128)} %param.13) | non-fusion elementwise | flops 8388608 | bytes 50331648 | tf_op jit(solution)/shard_map/convert_element_type | solution.py:20
  271.0 165.7 %all-to-all-done.1 = bf16[32,512,512]{2,1,0:T(8,128)(2,1)} async-done(((bf16[32,512,512]{2,1,0:T(8,128)(2,1)}), bf16[32,512,512]{2,1,0:T(8,128)(2,1)}, u32[]{:S(2)}, u32[]{:S(2)}) %all-to-all-start.1) | async-done | bytes 16777248 | tf_op jit(solution)/shard_map/all_to_all | solution.py:23
  436.7 7.0 %all-to-all-start.2 = ((bf16[32,512,512]{2,1,0:T(8,128)(2,1)}), bf16[32,512,512]{2,1,0:T(8,128)(2,1)}, u32[]{:S(2)}, u32[]{:S(2)}) async-start(bf16[32,512,512]{2,1,0:T(8,128)(2,1)} %convert_element_type.41), calls=%async_computation.2 | async-start | bytes 33554432 | tf_op jit(solution)/shard_map/all_to_all | solution.py:24
  443.6 0.0 all-gather.3.cloned.1.call-start
  443.7 0.8 copy.45
  444.6 0.0 all-gather.5.cloned.1.call-start
  444.6 13.8 %copy.38 = bf16[4,8,512,512]{3,2,0,1:T(8,128)(2,1)} copy(bf16[4,8,512,512]{3,2,1,0:T(8,128)(2,1)} %bitcast.59) | data formatting | bytes 33554432 | tf_op jit(solution)/shard_map/all_to_all | solution.py:22
  458.4 13.8 %copy.39 = bf16[4,8,512,512]{3,2,0,1:T(8,128)(2,1)} copy(bf16[4,8,512,512]{3,2,1,0:T(8,128)(2,1)} %bitcast.3) | data formatting | bytes 33554432 | tf_op jit(solution)/shard_map/all_to_all | solution.py:23
  472.3 22.4 %all-gather.3.cloned.1.call-done = bf16[4,8,16,2048]{3,2,0,1:T(8,128)(2,1)} async-done(((bf16[4,8,16,512]{3,2,0,1:T(8,128)(2,1)}), bf16[4,8,16,2048]{3,2,0,1:T(8,128)(2,1)}) %all-gather.3.cloned.1.call-update) | async-done | bytes 2097168 | tf_op jit(solution)/shard_map/all_gather | solution.py:57
  494.7 9.3 %fusion = f32[4,8,16,512]{3,2,0,1:T(8,128)S(1)} fusion(bf16[8,2048,512,1]{2,1,3,0:T(8,128)(2,1)} %bitcast.62, bf16[4,8,16,2048]{3,2,0,1:T(8,128)(2,1)} %all-gather.3.cloned.1.call-done), kind=kOutput, calls=%fused_computation.3 | convolution fusion | flops 1074003968 | bytes 19922944 | tf_op jit(solution)/shard_map/secd,edf->secf/dot_general | solution.py:58
  504.0 8.4 %fusion.4 = bf16[4,8,16,512]{3,2,0,1:T(8,128)(2,1)} fusion(bf16[8,2048,512,1]{2,1,3,0:T(8,128)(2,1)} %bitcast.64, bf16[4,8,16,2048]{3,2,0,1:T(8,128)(2,1)S(1)} %copy-done, f32[4,8,16,512]{3,2,0,1:T(8,128)S(1)} %fusion), kind=kOutput, calls=%fused_computation.10 | convolution fusion | flops 1076101120 | bytes 20447232 | tf_op jit(solution)/shard_map/secd,edf->secf/dot_general | solution.py:61
  512.4 114.3 %all-to-all-done.2 = bf16[32,512,512]{2,1,0:T(8,128)(2,1)} async-done(((bf16[32,512,512]{2,1,0:T(8,128)(2,1)}), bf16[32,512,512]{2,1,0:T(8,128)(2,1)}, u32[]{:S(2)}, u32[]{:S(2)}) %all-to-all-start.2) | async-done | bytes 16777248 | tf_op jit(solution)/shard_map/all_to_all | solution.py:24
  626.7 13.8 %copy.40 = bf16[4,8,512,512]{3,2,0,1:T(8,128)(2,1)} copy(bf16[4,8,512,512]{3,2,1,0:T(8,128)(2,1)} %bitcast.6) | data formatting | bytes 33554432 | tf_op jit(solution)/shard_map/all_to_all | solution.py:24
  640.5 9.3 %fusion.5 = bf16[4,8,16,512]{3,2,0,1:T(8,128)(2,1)S(1)} fusion(bf16[4,8,16,2048]{3,2,0,1:T(8,128)(2,1)} %all-gather.5.cloned.1.call-done, bf16[8,2048,512,1]{2,1,3,0:T(8,128)(2,1)} %bitcast.60), kind=kOutput, calls=%fused_computation.11 | convolution fusion | flops 1074003968 | bytes 19398656 | tf_op jit(solution)/shard_map/secf,efd->secd/dot_general | solution.py:63
  649.8 11.2 %all_to_all.65 = bf16[32,16,512]{2,1,0:T(8,128)(2,1)S(1)} all-to-all(bf16[32,16,512]{2,1,0:T(8,128)(2,1)S(1)} %bitcast.68), channel_id=1, replica_groups=mesh['grp'=2,'fs'=4,'tp'=4] {'tp'}, dimensions={0} | all-to-all | bytes 1048576 | tf_op jit(solution)/shard_map/all_to_all | solution.py:70
  661.0 1.0 convolution_convert_fusion.2
  (13 shorter events, 0.2 us)
Async XLA Ops:
  15.0 37.4 %all-to-all-start.3 = ((bf16[32,16,512]{2,1,0:T(8,128)(2,1)}), bf16[32,16,512]{2,1,0:T(8,128)(2,1)S(1)}, u32[]{:S(2)}, u32[]{:S(2)}) async-start(bf16[32,16,512]{2,1,0:T(8,128)(2,1)} %bitcast.13), calls=%async_computation.3 | async-start | bytes 1048576 | tf_op jit(solution)/shard_map/all_to_all | solution.py:49
  246.6 190.1 %all-to-all-start.1 = ((bf16[32,512,512]{2,1,0:T(8,128)(2,1)}), bf16[32,512,512]{2,1,0:T(8,128)(2,1)}, u32[]{:S(2)}, u32[]{:S(2)}) async-start(bf16[32,512,512]{2,1,0:T(8,128)(2,1)} %get-tuple-element.6), calls=%async_computation.1 | async-start | bytes 33554432 | tf_op jit(solution)/shard_map/all_to_all | solution.py:23
  436.7 190.0 %all-to-all-start.2 = ((bf16[32,512,512]{2,1,0:T(8,128)(2,1)}), bf16[32,512,512]{2,1,0:T(8,128)(2,1)}, u32[]{:S(2)}, u32[]{:S(2)}) async-start(bf16[32,512,512]{2,1,0:T(8,128)(2,1)} %convert_element_type.41), calls=%async_computation.2 | async-start | bytes 33554432 | tf_op jit(solution)/shard_map/all_to_all | solution.py:24
  443.6 51.0 %all-gather.3.cloned.1.call-start = ((), (), s32[]{:S(2)}) async-start(), calls=%async_computation.5 | async-start | bytes 2621440 | tf_op jit(solution)/shard_map/all_gather | solution.py:57
  444.6 195.9 %all-gather.5.cloned.1.call-start = ((), (), s32[]{:S(2)}) async-start(), calls=%async_computation.6 | async-start | bytes 2621440 | tf_op jit(solution)/shard_map/all_gather | solution.py:65
  494.7 9.3 %copy-start = (bf16[4,8,16,2048]{3,2,0,1:T(8,128)(2,1)S(1)}, bf16[4,8,16,2048]{3,2,0,1:T(8,128)(2,1)}, u32[]{:S(2)}) copy-start(bf16[4,8,16,2048]{3,2,0,1:T(8,128)(2,1)} %all-gather.3.cloned.1.call-done) | copy-start | bytes 6291460
Sparse Core Ops, SparseCore 0:
  446.6 48.0 all-gather.2
  512.5 44.4 all-gather.4
where the time goes:
time: 670 us; the launch traced here: 669 us
  waiting for transfers between devices  302 us (45%)
  blocking collectives  205 us (31%)
  other arithmetic  55.9 us (8%)
  local copies, waits for them, and re-layouts  43.6 us (7%)
  matrix products  29.2 us (4%)
  starting transfers between devices  18.4 us (3%)
  between operations  14.2 us (2%)
    all_to_all x1, blocking collectives, local(): lax.all_to_all(gate_local, 'tp', split_axis=0, concat_axis=1, tiled=True)  194 us
    all_to_all x1, waiting for transfers between devices, local(): lax.all_to_all(up_local, 'tp', split_axis=0, concat_axis=1, tiled=True)  166 us
    all_to_all x1, waiting for transfers between devices, local(): lax.all_to_all(down_local, 'tp', split_axis=0, concat_axis=1, tiled=True)  114 us
    convert_element_type x1, other arithmetic, local(): up_local = (up_train * norm_gain[None, :, None]).astype(jnp.bfloat16)  33.2 us
    all_gather x1, waiting for transfers between devices, local(): block_in = lax.all_gather(arrived, 'fs', axis=3, tiled=True)  22.4 us
    convert_element_type x1, other arithmetic, local(): down_local = down_train.astype(jnp.bfloat16)  17.3 us
    all_to_all x1, local copies, waits for them, and re-layouts, local(): lax.all_to_all(gate_local, 'tp', split_axis=0, concat_axis=1, tiled=True)  13.8 us
    all_to_all x1, local copies, waits for them, and re-layouts, local(): lax.all_to_all(up_local, 'tp', split_axis=0, concat_axis=1, tiled=True)  13.8 us
  transfers between devices with their start and end apart: 5, of which 3 were waited for; matrix products, arithmetic and copies ran while one was open for 17% of the time, Pallas kernels for 0%

commit v1 on v0

--- a/solution.py
+++ b/solution.py
@@ -21,7 +21,12 @@
     gate_serve, up_serve, down_serve = (
         lax.all_to_all(gate_local, "tp", split_axis=0, concat_axis=1, tiled=True),
         lax.all_to_all(up_local, "tp", split_axis=0, concat_axis=1, tiled=True),
-        lax.all_to_all(down_local, "tp", split_axis=0, concat_axis=1, tiled=True),
+        jnp.concatenate(
+            lax.all_to_all(
+                jnp.stack(jnp.split(down_local, lax.axis_size("tp"), axis=0)), "tp", 0, 0
+            ),
+            axis=1,
+        ),
     )
     tp_count = lax.axis_size("tp")
     fs_count = lax.axis_size("fs")

time: 670 us -> 669 us (level)
  waiting for transfers between devices: 302 us -> 288 us
  other arithmetic: 55.9 us -> 64.3 us
    all_to_all x1, waiting for transfers between devices: 166 us -> 151 us  [local(): lax.all_to_all(up_local, 'tp', split_axis=0, concat_axis=1, tiled=True)]
    another operation x4 -> x5, other arithmetic: 1.3 us -> 15.1 us  [the longest x1 13.8 us: local(): jnp.stack(jnp.split(down_local, lax.axis_size('tp'), axis=0))]
    all_to_all x1 -> x0, local copies, waits for them, and re-layouts: 13.8 us -> none  [local(): lax.all_to_all(down_local, 'tp', split_axis=0, concat_axis=1, tiled=True)]
    reshape x0 -> x1, local copies, waits for them, and re-layouts: none -> 13.8 us  [local(): jnp.concatenate(lax.all_to_all(jnp.stack(jnp.split(down_local, lax.axis_s...]
  transfers between devices with their start and end apart: 5 -> 5, of which waited for: 3 -> 3; matrix products, arithmetic and copies ran while one was open for 17% -> 19% of each run, Pallas kernels for 0% -> 0%
where the time goes in v1:
time: 669 us; the launch traced here: 667 us
  waiting for transfers between devices  288 us (43%)
  blocking collectives  205 us (31%)
  other arithmetic  64.3 us (10%)
  local copies, waits for them, and re-layouts  49.7 us (7%)
  matrix products  27.7 us (4%)
  starting transfers between devices  18.4 us (3%)
  between operations  14.2 us (2%)
    all_to_all x1, blocking collectives, local(): lax.all_to_all(gate_local, 'tp', split_axis=0, concat_axis=1, tiled=True)  194 us
    all_to_all x1, waiting for transfers between devices, local(): lax.all_to_all(up_local, 'tp', split_axis=0, concat_axis=1, tiled=True)  151 us
    all_to_all x1, waiting for transfers between devices, local(): lax.all_to_all(jnp.stack(jnp.split(down_local, lax.axis_size('tp'), axis=...  114 us
    convert_element_type x1, other arithmetic, local(): up_local = (up_train * norm_gain[None, :, None]).astype(jnp.bfloat16)  33.2 us
    all_gather x1, waiting for transfers between devices, local(): block_in = lax.all_gather(arrived, 'fs', axis=3, tiled=True)  22.4 us
    all_to_all x1, local copies, waits for them, and re-layouts, local(): lax.all_to_all(gate_local, 'tp', split_axis=0, concat_axis=1, tiled=True)  13.8 us
    another operation x1, other arithmetic, local(): jnp.stack(jnp.split(down_local, lax.axis_size('tp'), axis=0))  13.8 us
    all_to_all x1, local copies, waits for them, and re-layouts, local(): lax.all_to_all(up_local, 'tp', split_axis=0, concat_axis=1, tiled=True)  13.8 us
  transfers between devices with their start and end apart: 5, of which 3 were waited for; matrix products, arithmetic and copies ran while one was open for 19% of the time, Pallas kernels for 0%

profile of v1, /device:TPU:0, one launch (start us, length us, event | category | flops | bytes accessed | tf_op | source)
XLA Modules:
  0.0 667.4 jit_solution(1817405561818624156)
XLA Ops:
  7.2 1.1 convert_element_type.44
  8.3 1.2 multiply_reduce_fusion
  9.5 0.8 copy.41
  10.3 0.1 eq.36
  10.5 1.2 reduce-window.6
  11.6 0.2 slice_reduce_fusion
  11.9 0.1 bitcast_bitcast_fusion
  12.0 0.1 reduce_sum.39
  12.1 0.1 copy.44
  12.2 0.7 multiply_add_fusion
  12.9 0.9 convert_reduce_fusion
  13.9 1.2 convolution_convert_fusion
  15.0 4.3 all-to-all-start.3
  19.3 33.2 %multiply_convert_fusion = (bf16[32,512,512]{2,1,0:T(8,128)(2,1)}, bf16[32,512,512]{2,1,0:T(8,128)(2,1)}) fusion(f32[32,512,512]{2,1,0:T(8,128)} %param.12, f32[512]{0:T(512)} %param.10, f32[32,512,512]{2,1,0:T(8,128)} %param.11), kind=kLoop, calls=%fused_computation | loop fusion | flops 33554432 | bytes 100665344 | tf_op jit(solution)/shard_map/convert_element_type | solution.py:19
  52.5 194.1 %all_to_all.51 = bf16[32,512,512]{2,1,0:T(8,128)(2,1)} all-to-all(bf16[32,512,512]{2,1,0:T(8,128)(2,1)} %get-tuple-element.11), channel_id=1, replica_groups=mesh['grp'=2,'fs'=4,'tp'=4] {'tp'}, dimensions={0} | all-to-all | bytes 33554432 | tf_op jit(solution)/shard_map/all_to_all | solution.py:22
  246.6 7.0 %all-to-all-start.1 = ((bf16[32,512,512]{2,1,0:T(8,128)(2,1)}), bf16[32,512,512]{2,1,0:T(8,128)(2,1)}, u32[]{:S(2)}, u32[]{:S(2)}) async-start(bf16[32,512,512]{2,1,0:T(8,128)(2,1)} %get-tuple-element.10), calls=%async_computation.1 | async-start | bytes 33554432 | tf_op jit(solution)/shard_map/all_to_all | solution.py:23
  253.5 11.9 %convert_element_type.41 = bf16[32,512,512]{2,1,0:T(8,128)(2,1)S(1)} convert(f32[32,512,512]{2,1,0:T(8,128)} %param.13) | non-fusion elementwise | flops 8388608 | bytes 50331648 | tf_op jit(solution)/shard_map/convert_element_type | solution.py:20
  265.5 6.1 slice_bitcast_fusion.3
  271.5 13.8 %pad_maximum_fusion = bf16[4,8,512,512]{3,2,1,0:T(8,128)(2,1)} fusion(bf16[1,8,512,512]{3,2,1,0:T(8,128)(2,1)} %get-tuple-element.7, bf16[1,8,512,512]{3,2,1,0:T(8,128)(2,1)} %get-tuple-element.8, bf16[1,8,512,512]{3,2,1,0:T(8,128)(2,1)} %get-tuple-element.9, bf16[1,8,512,512]{3,2,1,0:T(8,128)(2,1)} %get-tuple-element.6), kind=kLoop, calls=%fused_computation.2 | loop fusion | flops 25165824 | bytes 33554432 | tf_op jit(solution)/shard_map/stack | solution.py:26
  285.4 151.2 %all-to-all-done.1 = bf16[32,512,512]{2,1,0:T(8,128)(2,1)} async-done(((bf16[32,512,512]{2,1,0:T(8,128)(2,1)}), bf16[32,512,512]{2,1,0:T(8,128)(2,1)}, u32[]{:S(2)}, u32[]{:S(2)}) %all-to-all-start.1) | async-done | bytes 16777248 | tf_op jit(solution)/shard_map/all_to_all | solution.py:23
  436.5 7.1 %all-to-all-start.2 = ((bf16[4,8,512,512]{3,2,1,0:T(8,128)(2,1)}), bf16[4,8,512,512]{3,2,1,0:T(8,128)(2,1)}, u32[]{:S(2)}, u32[]{:S(2)}) async-start(bf16[4,8,512,512]{3,2,1,0:T(8,128)(2,1)} %pad_maximum_fusion), calls=%async_computation.2 | async-start | bytes 33554432 | tf_op jit(solution)/shard_map/all_to_all | solution.py:25
  443.7 0.8 copy.45
  444.6 13.8 %copy.38 = bf16[4,8,512,512]{3,2,0,1:T(8,128)(2,1)} copy(bf16[4,8,512,512]{3,2,1,0:T(8,128)(2,1)} %bitcast.65) | data formatting | bytes 33554432 | tf_op jit(solution)/shard_map/all_to_all | solution.py:22
  458.4 13.8 %copy.39 = bf16[4,8,512,512]{3,2,0,1:T(8,128)(2,1)} copy(bf16[4,8,512,512]{3,2,1,0:T(8,128)(2,1)} %bitcast.3) | data formatting | bytes 33554432 | tf_op jit(solution)/shard_map/all_to_all | solution.py:23
  472.2 22.4 %all-gather.3.cloned.1.call-done = bf16[4,8,16,2048]{3,2,0,1:T(8,128)(2,1)} async-done(((bf16[4,8,16,512]{3,2,0,1:T(8,128)(2,1)}), bf16[4,8,16,2048]{3,2,0,1:T(8,128)(2,1)}) %all-gather.3.cloned.1.call-update) | async-done | bytes 2097168 | tf_op jit(solution)/shard_map/all_gather | solution.py:62
  494.7 9.3 %fusion = f32[4,8,16,512]{3,2,0,1:T(8,128)S(1)} fusion(bf16[8,2048,512,1]{2,1,3,0:T(8,128)(2,1)} %bitcast.66, bf16[4,8,16,2048]{3,2,0,1:T(8,128)(2,1)} %all-gather.3.cloned.1.call-done), kind=kOutput, calls=%fused_computation.8 | convolution fusion | flops 1074003968 | bytes 19922944 | tf_op jit(solution)/shard_map/secd,edf->secf/dot_general | solution.py:63
  504.0 8.4 %fusion.4 = bf16[4,8,16,512]{3,2,0,1:T(8,128)(2,1)} fusion(bf16[8,2048,512,1]{2,1,3,0:T(8,128)(2,1)} %bitcast.68, bf16[4,8,16,2048]{3,2,0,1:T(8,128)(2,1)S(1)} %copy-done, f32[4,8,16,512]{3,2,0,1:T(8,128)S(1)} %fusion), kind=kOutput, calls=%fused_computation.15 | convolution fusion | flops 1076101120 | bytes 20447232 | tf_op jit(solution)/shard_map/secd,edf->secf/dot_general | solution.py:66
  512.4 114.3 %all-to-all-done.2 = bf16[4,8,512,512]{3,2,1,0:T(8,128)(2,1)} async-done(((bf16[4,8,512,512]{3,2,1,0:T(8,128)(2,1)}), bf16[4,8,512,512]{3,2,1,0:T(8,128)(2,1)}, u32[]{:S(2)}, u32[]{:S(2)}) %all-to-all-start.2) | async-done | bytes 16777248 | tf_op jit(solution)/shard_map/all_to_all | solution.py:25
  626.6 13.8 %copy.40 = bf16[8,4,512,512]{3,2,1,0:T(8,128)(2,1)} copy(bf16[8,4,512,512]{3,2,0,1:T(8,128)(2,1)} %bitcast.10) | data formatting | bytes 33554432 | tf_op jit(solution)/shard_map/reshape | solution.py:24
  640.4 7.9 %fusion.5 = bf16[4,8,16,512]{3,2,0,1:T(8,128)(2,1)S(1)} fusion(bf16[8,2048,512,1]{2,1,3,0:T(8,128)(2,1)} %bitcast.70, bf16[4,8,16,2048]{3,2,0,1:T(8,128)(2,1)} %all-gather.5.cloned.1.call-done), kind=kOutput, calls=%fused_computation.16 | convolution fusion | flops 1074003968 | bytes 19398656 | tf_op jit(solution)/shard_map/secf,efd->secd/dot_general | solution.py:68
  648.4 11.2 %all_to_all.52 = bf16[32,16,512]{2,1,0:T(8,128)(2,1)S(1)} all-to-all(bf16[32,16,512]{2,1,0:T(8,128)(2,1)S(1)} %bitcast.74), channel_id=1, replica_groups=mesh['grp'=2,'fs'=4,'tp'=4] {'tp'}, dimensions={0} | all-to-all | bytes 1048576 | tf_op jit(solution)/shard_map/all_to_all | solution.py:75
  659.6 1.0 convolution_convert_fusion.2
  (15 shorter events, 0.3 us)
Async XLA Ops:
  15.0 37.4 %all-to-all-start.3 = ((bf16[32,16,512]{2,1,0:T(8,128)(2,1)}), bf16[32,16,512]{2,1,0:T(8,128)(2,1)S(1)}, u32[]{:S(2)}, u32[]{:S(2)}) async-start(bf16[32,16,512]{2,1,0:T(8,128)(2,1)} %bitcast.18), calls=%async_computation.3 | async-start | bytes 1048576 | tf_op jit(solution)/shard_map/all_to_all | solution.py:54
  246.6 190.0 %all-to-all-start.1 = ((bf16[32,512,512]{2,1,0:T(8,128)(2,1)}), bf16[32,512,512]{2,1,0:T(8,128)(2,1)}, u32[]{:S(2)}, u32[]{:S(2)}) async-start(bf16[32,512,512]{2,1,0:T(8,128)(2,1)} %get-tuple-element.10), calls=%async_computation.1 | async-start | bytes 33554432 | tf_op jit(solution)/shard_map/all_to_all | solution.py:23
  436.5 190.1 %all-to-all-start.2 = ((bf16[4,8,512,512]{3,2,1,0:T(8,128)(2,1)}), bf16[4,8,512,512]{3,2,1,0:T(8,128)(2,1)}, u32[]{:S(2)}, u32[]{:S(2)}) async-start(bf16[4,8,512,512]{3,2,1,0:T(8,128)(2,1)} %pad_maximum_fusion), calls=%async_computation.2 | async-start | bytes 33554432 | tf_op jit(solution)/shard_map/all_to_all | solution.py:25
  443.6 51.0 %all-gather.3.cloned.1.call-start = ((), (), s32[]{:S(2)}) async-start(), calls=%async_computation.5 | async-start | bytes 2621440 | tf_op jit(solution)/shard_map/all_gather | solution.py:62
  444.5 195.9 %all-gather.5.cloned.1.call-start = ((), (), s32[]{:S(2)}) async-start(), calls=%async_computation.6 | async-start | bytes 2621440 | tf_op jit(solution)/shard_map/all_gather | solution.py:70
  494.7 9.3 %copy-start = (bf16[4,8,16,2048]{3,2,0,1:T(8,128)(2,1)S(1)}, bf16[4,8,16,2048]{3,2,0,1:T(8,128)(2,1)}, u32[]{:S(2)}) copy-start(bf16[4,8,16,2048]{3,2,0,1:T(8,128)(2,1)} %all-gather.3.cloned.1.call-done) | copy-start | bytes 6291460
Sparse Core Ops, SparseCore 0:
  446.6 48.0 all-gather.2
  512.5 44.4 all-gather.4
